TPU v7x, 32 devices: a whole 2x2x4 slice. The times are simulated.
32 devices in a mesh: sp: 16 (over z, y, core), tp: 2 (over x).
Axes of the slice: x: 2, y: 2, z: 4, core: 2. Of those that a mesh axis runs over, the one named last changes fastest.
Arguments:
- queries: bfloat16 [8192, 1024], P('sp', 'tp'), may hold values from -260 to 260, as said below
- keys: bfloat16 [8192, 512], P('sp', 'tp'), may hold values from -8 to 8, as said below
- values: bfloat16 [8192, 512], P('sp', 'tp'), may hold values from -24 to 24
- doc_ids: int32 [8192], P('sp'), may hold values from 0 to 3, never falling along the last dimension, each value on 1 to 4096 neighbouring positions
- sink_logit: float32 [8], P('tp'), may hold values from 2 to 7
- residual_in: bfloat16 [8192, 2048], P(('sp', 'tp')), may hold values from -6 to 6
- w_out: bfloat16 [1024, 2048], replicated, may hold values from -0.375 to 0.375
- gain_one: float32 [2048], replicated, may hold values from 0.1 to 1.9
- w_gate: bfloat16 [2048, 5632], P('sp', 'tp'), may hold values from -0.125 to 0.125
- w_up: bfloat16 [2048, 5632], P('sp', 'tp'), may hold values from -0.125 to 0.125
- w_down: bfloat16 [5632, 2048], P('tp', 'sp'), may hold values from -0.078125 to 0.078125
- gain_two: float32 [2048], replicated, may hold values from 0.1 to 1.9
Outputs:
- layer_out: bfloat16 [8192, 2048], P(('sp', 'tp'))
Inputs may be any that keep to these rules, and one draw needn't show every extreme that they name: Real-valued projected queries. Real-valued projected keys. `doc_ids`: document numbers never fall along the sequence; each document is one run of positions.
All inputs are finite; a program needn't handle non-finite values.
Results may differ from a plain program's by a relative error of at most 0.012.
Values may be sent and summed in bfloat16 or wider, within the bound.
A program may use at most 128 MiB of HBM per device.

v0:
```python
import math
import jax
import jax.numpy as jnp
from jax import lax
from jax.sharding import PartitionSpec as P

HEAD = 128
HALF = 128
ALPHA = 2.0**0.5
EPS = 1e-05
NEGATIVE = -1e30


def shifted(value, axis, steps):
    count = lax.axis_size(axis)
    leading, last = (max(0, -steps), min(count, count - steps))
    return lax.ppermute(value, axis, [(source, source + steps) for source in range(leading, last)])


def layer_norm(values_in, gain):
    average = jnp.mean(values_in, -1, keepdims=True)
    centred = values_in - average
    variance = jnp.mean(centred * centred, -1, keepdims=True)
    return centred * lax.rsqrt(variance + EPS) * gain


def per_device(
    queries,
    keys,
    values,
    doc_ids,
    sink_logit,
    residual_in,
    w_out,
    gain_one,
    w_gate,
    w_up,
    w_down,
    gain_two,
):
    row_count = queries.shape[0]
    sp_size = lax.axis_size("sp")
    kv_local = keys.shape[1] // HEAD
    repeat = queries.shape[1] // keys.shape[1]
    lower = (keys[row_count - HALF :], values[row_count - HALF :], doc_ids[row_count - HALF :])
    upper = (keys[:HALF], values[:HALF], doc_ids[:HALF])
    before = shifted((lower[0], lower[1], lower[2]), "sp", 1)
    after = shifted((upper[0], upper[1], upper[2]), "sp", -1)
    keys_all = jnp.concatenate([before[0], keys, after[0]], 0)
    values_all = jnp.concatenate([before[1], values, after[1]], 0)
    docs_all = jnp.concatenate([before[2], doc_ids, after[2]], 0)
    first_pos = lax.axis_index("sp") * row_count
    block = math.gcd(512, row_count)
    span = block + 2 * HALF
    sinks = sink_logit.reshape(kv_local, repeat)

    def one_block(index):
        start = index * block
        query_blk = queries.reshape(block, kv_local, repeat, HEAD)
        key_blk = keys_all.reshape(span, kv_local, HEAD)
        value_blk = values_all.reshape(span, kv_local, HEAD)
        pos_query = first_pos + start + jnp.arange(block, dtype=jnp.int32)
        pos_key = first_pos + start - HALF + jnp.arange(span, dtype=jnp.int32)
        offset = pos_key[None, :] - pos_query[:, None]
        allowed = (jnp.abs(offset) <= HALF) & (docs_all[None, :] == doc_ids[:, None])
        allowed = allowed & (pos_key[None, :] >= 0) & (pos_key[None, :] < sp_size * row_count)
        scores = jnp.einsum(
            "qgrd,kgd->grqk", query_blk, key_blk, preferred_element_type=jnp.float32
        ) * HEAD ** (-0.5)
        scores = jnp.where(allowed[None, None], scores, NEGATIVE)
        top = jnp.maximum(jnp.max(scores, -1), sinks[:, :, None])
        weights = jnp.exp(scores - top[..., None])
        total = jnp.sum(weights, -1) + jnp.exp(sinks[:, :, None] - top)
        summed = jnp.einsum(
            "grqk,kgd->qgrd",
            weights.astype(jnp.bfloat16),
            value_blk,
            preferred_element_type=jnp.float32,
        )
        scaled = summed / jnp.transpose(total, (2, 0, 1))[..., None]
        return scaled.reshape(block, kv_local * repeat * HEAD).astype(jnp.bfloat16)

    attended = lax.map(one_block, jnp.arange(row_count // block, dtype=jnp.int32)).reshape(
        row_count, -1
    )
    token_rows = lax.all_to_all(attended, "tp", split_axis=0, concat_axis=1, tiled=True)
    mixed_rows = jnp.dot(token_rows, w_out, preferred_element_type=jnp.float32)
    pre_one = ALPHA * residual_in.astype(jnp.float32) + mixed_rows
    normed = layer_norm(pre_one, gain_one).astype(jnp.bfloat16)
    whole_rows = lax.all_gather(normed, "tp", axis=0, tiled=True)
    gate_whole, up_whole = (
        lax.all_gather(w_gate, "sp", axis=0, tiled=True),
        lax.all_gather(w_up, "sp", axis=0, tiled=True),
    )
    gate_part = jnp.dot(whole_rows, gate_whole, preferred_element_type=jnp.float32)
    up_part = jnp.dot(whole_rows, up_whole, preferred_element_type=jnp.float32)
    hidden = (jax.nn.silu(gate_part) * up_part).astype(jnp.bfloat16)
    down_terms = jnp.dot(
        hidden, lax.all_gather(w_down, "sp", axis=1, tiled=True), preferred_element_type=jnp.float32
    )
    rounded = lax.optimization_barrier(down_terms.astype(jnp.bfloat16)).astype(jnp.float32)
    down_rows = lax.psum_scatter(
        rounded.astype(jnp.bfloat16), "tp", scatter_dimension=0, tiled=True
    ).astype(jnp.float32)
    pre_two = ALPHA * normed.astype(jnp.float32) + down_rows
    return layer_norm(pre_two, gain_two).astype(jnp.bfloat16)


def solution(mesh):
    in_specs = (
        P("sp", "tp"),
        P("sp", "tp"),
        P("sp", "tp"),
        P("sp"),
        P("tp"),
        P(("sp", "tp"), None),
        P(),
        P(),
        P("sp", "tp"),
        P("sp", "tp"),
        P("tp", "sp"),
        P(),
    )
    out_specs = P(("sp", "tp"), None)
    return jax.shard_map(
        per_device, mesh=mesh, in_specs=in_specs, out_specs=out_specs, check_vma=False
    )
```

profile of v0, /device:TPU:0, one launch (start us, length us, event | category | flops | bytes accessed | tf_op | source)
XLA Modules:
  0.0 442.6 jit_solution(3270424816436045704)
XLA Ops:
  6.5 0.0 copy-start.5
  6.5 0.0 copy-start.7
  6.5 0.0 all-gather.5.cloned.1.call-start
  6.5 0.8 fusion.24
  7.3 2.4 collective-permute-start.2
  9.7 1.3 collective-permute-start.3
  11.0 1.1 copy.17
  12.1 5.2 %collective-permute-start.4 = (bf16[128,256]{0,1:T(8,128)(2,1)S(1)}, bf16[128,256]{0,1:T(8,128)(2,1)S(1)}, u32[]{:S(2)}, u32[]{:S(2)}) collective-permute-start(bf16[128,256]{0,1:T(8,128)(2,1)S(1)} %get-tuple-element.21), channel_id=1, source_target_pairs={{0,2},{2,4},{4,6},{6,8},{8,10},{10,12},{12,14},{14,16},{16,18},{18... | collective-permute-start | bytes 196616 | tf_op jit(solution)/shard_map/ppermute | solution.py:17
  17.3 1.3 collective-permute-start.5
  18.6 0.9 fusion.23
  19.5 4.3 collective-permute-start
  23.8 1.2 reshape.158
  25.0 0.0 copy-done.7
  25.0 0.1 max.20
  25.1 0.0 collective-permute-done.2
  25.1 1.3 collective-permute-start.1
  26.4 0.0 collective-permute-done.3
  26.4 0.0 copy-done.5
  26.4 0.9 fusion.9
  27.4 0.0 collective-permute-done.4
  27.4 0.0 collective-permute-done.5
  27.4 1.4 fusion.2
  28.9 0.0 copy-start.1
  28.9 0.1 broadcast_maximum_fusion
  29.0 0.0 copy-start.3
  29.0 1.4 fusion
  30.3 1.2 copy-done.1
  31.5 0.1 add_bitcast_fusion
  31.6 0.0 collective-permute-done
  31.6 0.0 collective-permute-done.1
  31.6 0.0 copy-done.3
  31.7 0.2 copy.16
  31.8 4.7 %divide_convert_fusion = bf16[512,2,2,128]{0,3,2,1:T(8,128)(2,1)S(1)} fusion(bf16[768,2,128,1]{0,2,3,1:T(8,128)(2,1)S(1)} %bitcast.47, f32[2,768,512,2]{2,1,3,0:T(8,128)} %copy-done.1, f32[2,2,512]{2,1,0:T(2,128)S(1)} %broadcast_maximum_fusion, pred[512,768]{0,1:T(8,128)(4,1)S(1)} %fusion.9, f32[512,2,2]{0,2,1:T(2,128)S(1)} %add_bitcast_fusion), kind=kOutput, calls=%fused_computation.21 | convolution fusion | flops 409468928 | bytes 7618560 | tf_op jit(solution)/shard_map/while/body/eval_jaxpr/grqk,kgd->qgrd/dot_general | solution.py:74
  36.5 0.0 copy-start.2
  36.6 0.1 convert_element_type.39
  36.7 0.1 copy.23
  36.8 10.8 %all_to_all.16 = bf16[2,256,512]{1,2,0:T(8,128)(2,1)S(1)} all-to-all(bf16[2,256,512]{1,2,0:T(8,128)(2,1)S(1)} %copy.23), channel_id=1, replica_groups=mesh['sp'=16,'tp'=2] {'tp'}, dimensions={0} | all-to-all | bytes 1048576 | tf_op jit(solution)/shard_map/all_to_all | solution.py:86
  47.6 0.0 copy-done.2
  47.6 3.6 fusion.25
  51.2 0.3 multiply_reduce_fusion.1
  51.5 0.3 copy-done.4
  51.9 1.3 multiply_convert_fusion.2
  53.2 0.0 all-gather.5.cloned.1.call-update
  53.2 0.0 all-gather.7.cloned.1.call-start
  53.3 0.7 all-gather.7.cloned.1.call-update
  54.0 0.0 all-gather.11.cloned.1.call-start
  54.0 0.7 all-gather.11.cloned.1.call-update
  54.7 0.0 all-gather.9.cloned.1.call-start
  54.7 0.5 all-gather.9.cloned.1.call-update
  55.3 0.0 reduce-scatter.2.cloned.1.call-start
  55.3 34.1 %all-gather.5.cloned.1.call-done = bf16[512,2048]{1,0:T(8,128)(2,1)} async-done(((bf16[256,2048]{1,0:T(8,128)(2,1)}), bf16[512,2048]{1,0:T(8,128)(2,1)}) %all-gather.5.cloned.1.call-update) | async-done | bytes 2097168 | tf_op jit(solution)/shard_map/all_gather | solution.py:90
  89.4 96.3 %all-gather.7.cloned.1.call-done = bf16[2048,2816]{1,0:T(8,128)(2,1)} async-done(((bf16[128,2816]{1,0:T(8,128)(2,1)}), bf16[2048,2816]{1,0:T(8,128)(2,1)}) %all-gather.7.cloned.1.call-update) | async-done | bytes 11534352 | tf_op jit(solution)/shard_map/all_gather | solution.py:92
  185.7 12.5 %fusion.26 = f32[512,2816]{1,0:T(8,128)} fusion(bf16[512,2048]{1,0:T(8,128)(2,1)} %all-gather.5.cloned.1.call-done, bf16[2048,2816]{1,0:T(8,128)(2,1)} %all-gather.7.cloned.1.call-done), kind=kOutput, calls=%fused_computation.44 | convolution fusion | flops 5905580032 | bytes 19398656 | tf_op jit(solution)/shard_map/dot_general | solution.py:95
  198.2 84.9 %all-gather.11.cloned.1.call-done = bf16[2816,2048]{1,0:T(8,128)(2,1)} async-done(((bf16[2816,128]{1,0:T(8,128)(2,1)}), bf16[2816,2048]{1,0:T(8,128)(2,1)}) %all-gather.11.cloned.1.call-update) | async-done | bytes 11534352 | tf_op jit(solution)/shard_map/all_gather | solution.py:99
  283.1 94.3 %all-gather.9.cloned.1.call-done = bf16[2048,2816]{1,0:T(8,128)(2,1)} async-done(((bf16[128,2816]{1,0:T(8,128)(2,1)}), bf16[2048,2816]{1,0:T(8,128)(2,1)}) %all-gather.9.cloned.1.call-update) | async-done | bytes 11534352 | tf_op jit(solution)/shard_map/all_gather | solution.py:93
  377.4 23.3 %convolution_convert_fusion = bf16[512,2048]{1,0:T(8,128)(2,1)} fusion(bf16[2816,2048]{1,0:T(8,128)(2,1)} %all-gather.11.cloned.1.call-done, f32[512,2816]{1,0:T(8,128)} %fusion.26, bf16[512,2048]{1,0:T(8,128)(2,1)} %all-gather.5.cloned.1.call-done, bf16[2048,2816]{1,0:T(8,128)(2,1)} %all-gather.9.cloned.1.call-done), kind=kOutput, calls=%fused_computation.8 | convolution fusion | flops 11820859392 | bytes 33030144 | tf_op jit(solution)/shard_map/dot_general | solution.py:98
  400.7 0.0 reduce-scatter.2.cloned.1.call-update
  400.7 30.3 %reduce-scatter.2.cloned.1.call-done = bf16[256,2048]{1,0:T(8,128)(2,1)} async-done(((bf16[512,2048]{1,0:T(8,128)(2,1)}), bf16[256,2048]{1,0:T(8,128)(2,1)}) %reduce-scatter.2.cloned.1.call-update) | async-done | bytes 1048592 | tf_op jit(solution)/shard_map/reduce_scatter | solution.py:102
  431.0 1.9 fusion.6
  433.0 0.0 copy-start.6
  433.0 0.0 copy-done
  433.0 0.8 multiply_reduce_fusion
  433.8 0.0 copy-done.6
  433.8 2.3 multiply_convert_fusion.1
  (13 shorter events, 0.1 us)
Async XLA Ops:
  6.5 19.9 %copy-start.5 = (s32[512]{0:T(512)S(1)}, s32[512]{0:T(512)}, u32[]{:S(2)}) copy-start(s32[512]{0:T(512)} %param.15) | copy-start | bytes 6148
  6.5 18.5 %copy-start.7 = (f32[4]{0:T(128)S(1)}, f32[4]{0:T(128)}, u32[]{:S(2)}) copy-start(f32[4]{0:T(128)} %param.16) | copy-start | bytes 52
  6.5 82.9 %all-gather.5.cloned.1.call-start = ((), (), s32[]{:S(2)}) async-start(), calls=%async_computation.2 | async-start | bytes 3145728 | tf_op jit(solution)/shard_map/all_gather | solution.py:90
  7.3 17.8 %collective-permute-start.2 = (s32[128]{0:T(128)S(1)}, s32[128]{0:T(128)S(1)}, u32[]{:S(2)}, u32[]{:S(2)}) collective-permute-start(s32[128]{0:T(128)S(1)} %get-tuple-element.25), channel_id=1, source_target_pairs={{0,2},{2,4},{4,6},{6,8},{8,10},{10,12},{12,14},{14,16},{16,18},{18... | collective-permute-start | bytes 1544 | tf_op jit(solution)/shard_map/ppermute | solution.py:17
  9.7 16.7 %collective-permute-start.3 = (s32[128]{0:T(128)S(1)}, s32[128]{0:T(128)S(1)}, u32[]{:S(2)}, u32[]{:S(2)}) collective-permute-start(s32[128]{0:T(128)S(1)} %get-tuple-element.26), channel_id=1, source_target_pairs={{2,0},{4,2},{6,4},{8,6},{10,8},{12,10},{14,12},{16,14},{18,16},{20... | collective-permute-start | bytes 1544 | tf_op jit(solution)/shard_map/ppermute | solution.py:17
  12.1 15.2 %collective-permute-start.4 = (bf16[128,256]{0,1:T(8,128)(2,1)S(1)}, bf16[128,256]{0,1:T(8,128)(2,1)S(1)}, u32[]{:S(2)}, u32[]{:S(2)}) collective-permute-start(bf16[128,256]{0,1:T(8,128)(2,1)S(1)} %get-tuple-element.21), channel_id=1, source_target_pairs={{0,2},{2,4},{4,6},{6,8},{8,10},{10,12},{12,14},{14,16},{16,18},{18... | collective-permute-start | bytes 196616 | tf_op jit(solution)/shard_map/ppermute | solution.py:17
  17.3 10.1 %collective-permute-start.5 = (bf16[128,256]{0,1:T(8,128)(2,1)S(1)}, bf16[128,256]{0,1:T(8,128)(2,1)S(1)}, u32[]{:S(2)}, u32[]{:S(2)}) collective-permute-start(bf16[128,256]{0,1:T(8,128)(2,1)S(1)} %get-tuple-element.22), channel_id=1, source_target_pairs={{2,0},{4,2},{6,4},{8,6},{10,8},{12,10},{14,12},{16,14},{18,16},{20... | collective-permute-start | bytes 196616 | tf_op jit(solution)/shard_map/ppermute | solution.py:17
  19.5 12.1 %collective-permute-start = (bf16[128,256]{1,0:T(8,128)(2,1)S(1)}, bf16[128,256]{1,0:T(8,128)(2,1)S(1)}, u32[]{:S(2)}, u32[]{:S(2)}) collective-permute-start(bf16[128,256]{1,0:T(8,128)(2,1)S(1)} %get-tuple-element.23), channel_id=1, source_target_pairs={{0,2},{2,4},{4,6},{6,8},{8,10},{10,12},{12,14},{14,16},{16,18},{18... | collective-permute-start | bytes 196616 | tf_op jit(solution)/shard_map/ppermute | solution.py:17
  25.1 6.5 %collective-permute-start.1 = (bf16[128,256]{1,0:T(8,128)(2,1)S(1)}, bf16[128,256]{1,0:T(8,128)(2,1)S(1)}, u32[]{:S(2)}, u32[]{:S(2)}) collective-permute-start(bf16[128,256]{1,0:T(8,128)(2,1)S(1)} %get-tuple-element.24), channel_id=1, source_target_pairs={{2,0},{4,2},{6,4},{8,6},{10,8},{12,10},{14,12},{16,14},{18,16},{20... | collective-permute-start | bytes 196616 | tf_op jit(solution)/shard_map/ppermute | solution.py:17
  28.9 2.6 copy-start.1
  29.0 2.7 copy-start.3
  36.5 11.1 %copy-start.2 = (bf16[256,2048]{1,0:T(8,128)(2,1)S(1)}, bf16[256,2048]{1,0:T(8,128)(2,1)}, u32[]{:S(2)}) copy-start(bf16[256,2048]{1,0:T(8,128)(2,1)} %param.17) | copy-start | bytes 3145732
  51.1 0.7 copy-start.4
  53.2 132.5 %all-gather.7.cloned.1.call-start = ((), (), s32[]{:S(2)}) async-start(), calls=%async_computation.3 | async-start | bytes 12255232 | tf_op jit(solution)/shard_map/all_gather | solution.py:92
  54.0 229.1 %all-gather.11.cloned.1.call-start = ((), (), s32[]{:S(2)}) async-start(), calls=%async_computation.5 | async-start | bytes 12255232 | tf_op jit(solution)/shard_map/all_gather | solution.py:99
  54.7 322.7 %all-gather.9.cloned.1.call-start = ((), (), s32[]{:S(2)}) async-start(), calls=%async_computation.4 | async-start | bytes 12255232 | tf_op jit(solution)/shard_map/all_gather | solution.py:93
  55.3 375.8 %reduce-scatter.2.cloned.1.call-start = ((), (), s32[]{:S(2)}) async-start(), calls=%async_computation.6 | async-start | bytes 3145728 | tf_op jit(solution)/shard_map/reduce_scatter | solution.py:102
  431.0 2.0 copy-start
  433.0 0.8 copy-start.6
Sparse Core Ops, SparseCore 0:
  53.3 36.0 all-gather.4
  91.7 93.9 all-gather.6
  187.9 95.1 all-gather.10
  285.2 92.1 all-gather.8
  400.8 30.1 reduce-scatter.1
where the time goes:
time: 443 us
  waiting for transfers between devices  342 us (77%)
  matrix products  45.5 us (10%)
  starting transfers between devices  15.8 us (4%)
  between operations  13.4 us (3%)
  blocking collectives  10.8 us (2%)
  other arithmetic  9.3 us (2%)
  local copies, waits for them, and re-layouts  5.92 us (1%)
    all_gather x1, waiting for transfers between devices, per_device(): lax.all_gather(w_gate, 'sp', axis=0, tiled=True)  96.3 us
    all_gather x1, waiting for transfers between devices, per_device(): lax.all_gather(w_up, 'sp', axis=0, tiled=True)  94.3 us
    all_gather x1, waiting for transfers between devices, per_device(): lax.all_gather(w_down, 'sp', axis=1, tiled=True)  84.9 us
    all_gather x1, waiting for transfers between devices, per_device(): whole_rows = lax.all_gather(normed, 'tp', axis=0, tiled=True)  34.1 us
    reduce_scatter x1, waiting for transfers between devices, per_device(): lax.psum_scatter(rounded.astype(jnp.bfloat16), 'tp', scatter_dimension=0,...  30.3 us
    dot_general x1, matrix products, per_device(): jnp.dot(hidden, lax.all_gather(w_down, 'sp', axis=1, tiled=True), preferr...  23.3 us
    ppermute x6, starting transfers between devices, shifted(): lax.ppermute(value, axis, [(source, source + steps) for source in range(l...  15.7 us
    dot_general x1, matrix products, per_device(): jnp.dot(whole_rows, gate_whole, preferred_element_type=jnp.float32)  12.5 us
  transfers between devices with their start and end apart: 11, of which 5 were waited for; matrix products, arithmetic and copies ran while one was open for 4% of the time, Pallas kernels for 0%

commit v1 on v0

--- a/solution.py
+++ b/solution.py
@@ -9,6 +9,12 @@
 ALPHA = 2.0**0.5
 EPS = 1e-05
 NEGATIVE = -1e30
+
+
+def all_parts(x, mesh_axis, d):
+    blocks = lax.all_gather(x, mesh_axis, axis=0, tiled=False)
+    out = jnp.concatenate(blocks, axis=d)
+    return out
 
 
 def shifted(value, axis, steps):
@@ -95,9 +101,7 @@
     gate_part = jnp.dot(whole_rows, gate_whole, preferred_element_type=jnp.float32)
     up_part = jnp.dot(whole_rows, up_whole, preferred_element_type=jnp.float32)
     hidden = (jax.nn.silu(gate_part) * up_part).astype(jnp.bfloat16)
-    down_terms = jnp.dot(
-        hidden, lax.all_gather(w_down, "sp", axis=1, tiled=True), preferred_element_type=jnp.float32
-    )
+    down_terms = jnp.dot(hidden, all_parts(w_down, "sp", 1), preferred_element_type=jnp.float32)
     rounded = lax.optimization_barrier(down_terms.astype(jnp.bfloat16)).astype(jnp.float32)
     down_rows = lax.psum_scatter(
         rounded.astype(jnp.bfloat16), "tp", scatter_dimension=0, tiled=True

time: 443 us -> 401 us (0.905)
  waiting for transfers between devices: 342 us -> 286 us
  local copies, waits for them, and re-layouts: 5.92 us -> 18.9 us
    all_gather x1, waiting for transfers between devices: 84.9 us -> 55.8 us  [all_parts(): blocks = lax.all_gather(x, mesh_axis, axis=0, tiled=False)]
    all_gather x1, waiting for transfers between devices: 34.1 us -> 17.7 us  [per_device(): whole_rows = lax.all_gather(normed, 'tp', axis=0, tiled=True)]
    reshape x0 -> x1, local copies, waits for them, and re-layouts: none -> 15.2 us  [all_parts(): out = jnp.concatenate(blocks, axis=d)]
    all_gather x1, waiting for transfers between devices: 94.3 us -> 81.9 us  [per_device(): lax.all_gather(w_up, 'sp', axis=0, tiled=True)]
  transfers between devices with their start and end apart: 11 -> 11, of which waited for: 5 -> 6; matrix products, arithmetic and copies ran while one was open for 4% -> 11% of each run, Pallas kernels for 0% -> 0%
where the time goes in v1:
time: 401 us; the launch traced here: 400 us
  waiting for transfers between devices  286 us (71%)
  matrix products  46.7 us (12%)
  local copies, waits for them, and re-layouts  18.9 us (5%)
  starting transfers between devices  16.1 us (4%)
  between operations  13.4 us (3%)
  blocking collectives  9.82 us (2%)
  other arithmetic  9.31 us (2%)
    all_gather x1, waiting for transfers between devices, per_device(): lax.all_gather(w_gate, 'sp', axis=0, tiled=True)  96.3 us
    all_gather x1, waiting for transfers between devices, per_device(): lax.all_gather(w_up, 'sp', axis=0, tiled=True)  81.9 us
    all_gather x1, waiting for transfers between devices, all_parts(): blocks = lax.all_gather(x, mesh_axis, axis=0, tiled=False)  55.8 us
    reduce_scatter x1, waiting for transfers between devices, per_device(): lax.psum_scatter(rounded.astype(jnp.bfloat16), 'tp', scatter_dimension=0,...  30.2 us
    dot_general x1, matrix products, per_device(): jnp.dot(hidden, all_parts(w_down, 'sp', 1), preferred_element_type=jnp.fl...  27.2 us
    all_gather x1, waiting for transfers between devices, per_device(): whole_rows = lax.all_gather(normed, 'tp', axis=0, tiled=True)  17.7 us
    ppermute x6, starting transfers between devices, shifted(): lax.ppermute(value, axis, [(source, source + steps) for source in range(l...  15.7 us
    reshape x1, local copies, waits for them, and re-layouts, all_parts(): out = jnp.concatenate(blocks, axis=d)  15.2 us
  transfers between devices with their start and end apart: 11, of which 6 were waited for; matrix products, arithmetic and copies ran while one was open for 11% of the time, Pallas kernels for 0%

profile of v1, /device:TPU:0, one launch (start us, length us, event | category | flops | bytes accessed | tf_op | source)
XLA Modules:
  0.0 400.1 jit_solution(16999408934687025760)
XLA Ops:
  6.5 0.0 copy-start.5
  6.5 0.0 copy-start.2
  6.5 0.0 copy-start.3
  6.5 0.0 all-gather.12.cloned.1.call-start
  6.6 0.7 all-gather.12.cloned.1.call-update
  7.3 0.0 all-gather.6.cloned.1.call-start
  7.3 0.8 fusion.24
  8.1 2.4 collective-permute-start.2
  10.5 1.3 collective-permute-start.3
  11.8 1.1 copy.25
  12.9 5.2 %collective-permute-start.4 = (bf16[128,256]{0,1:T(8,128)(2,1)S(1)}, bf16[128,256]{0,1:T(8,128)(2,1)S(1)}, u32[]{:S(2)}, u32[]{:S(2)}) collective-permute-start(bf16[128,256]{0,1:T(8,128)(2,1)S(1)} %get-tuple-element.21), channel_id=1, source_target_pairs={{0,2},{2,4},{4,6},{6,8},{8,10},{10,12},{12,14},{14,16},{16,18},{18... | collective-permute-start | bytes 196616 | tf_op jit(solution)/shard_map/ppermute | solution.py:23
  18.1 1.3 collective-permute-start.5
  19.4 0.9 fusion.23
  20.3 4.3 %collective-permute-start = (bf16[128,256]{1,0:T(8,128)(2,1)S(1)}, bf16[128,256]{1,0:T(8,128)(2,1)S(1)}, u32[]{:S(2)}, u32[]{:S(2)}) collective-permute-start(bf16[128,256]{1,0:T(8,128)(2,1)S(1)} %get-tuple-element.23), channel_id=1, source_target_pairs={{0,2},{2,4},{4,6},{6,8},{8,10},{10,12},{12,14},{14,16},{16,18},{18... | collective-permute-start | bytes 196616 | tf_op jit(solution)/shard_map/ppermute | solution.py:23
  24.6 0.0 copy-done.3
  24.6 0.1 reshape.164
  24.7 0.0 copy-done.7
  24.8 0.1 max.20
  24.8 0.0 collective-permute-done.2
  24.8 1.3 collective-permute-start.1
  26.1 0.0 collective-permute-done.3
  26.1 0.0 copy-done.5
  26.2 0.9 fusion.9
  27.1 0.0 collective-permute-done
  27.1 2.1 collective-permute-done.1
  29.2 0.0 copy-done.2
  29.2 0.2 copy.24
  29.4 0.0 collective-permute-done.4
  29.4 0.0 collective-permute-done.5
  29.5 1.4 fusion.2
  30.9 0.1 broadcast_maximum_fusion
  31.0 1.4 fusion
  32.4 0.1 add_bitcast_fusion
  32.5 2.0 divide_convert_fusion
  34.5 0.0 copy-start.1
  34.5 0.1 convert_element_type.39
  34.6 0.1 copy.31
  34.7 9.8 %all_to_all.16 = bf16[2,256,512]{1,2,0:T(8,128)(2,1)S(1)} all-to-all(bf16[2,256,512]{1,2,0:T(8,128)(2,1)S(1)} %copy.31), channel_id=1, replica_groups=mesh['sp'=16,'tp'=2] {'tp'}, dimensions={0} | all-to-all | bytes 1048576 | tf_op jit(solution)/shard_map/all_to_all | solution.py:92
  44.5 0.0 copy-done.1
  44.5 3.6 fusion.25
  48.1 0.4 multiply_reduce_fusion.1
  48.5 0.3 copy-done.4
  48.8 1.3 multiply_convert_fusion.2
  50.1 0.0 all-gather.6.cloned.1.call-update
  50.1 0.0 all-gather.8.cloned.1.call-start
  50.2 0.7 all-gather.8.cloned.1.call-update
  50.9 0.0 all-gather.10.cloned.1.call-start
  50.9 0.5 all-gather.10.cloned.1.call-update
  51.4 0.2 reduce-scatter.2.cloned.1.call-start
  51.7 55.8 %all-gather.12.cloned.1.call-done = bf16[45056,128]{1,0:T(8,128)(2,1)} async-done(((bf16[2816,128]{1,0:T(8,128)(2,1)}), bf16[45056,128]{1,0:T(8,128)(2,1)}) %all-gather.12.cloned.1.call-update) | async-done | bytes 11534352 | tf_op jit(solution)/shard_map/all_gather | solution.py:15
  107.4 15.2 %copy.32 = bf16[2816,16,128]{0,2,1:T(8,128)(2,1)} copy(bf16[2816,16,128]{2,0,1:T(8,128)(2,1)} %bitcast.49) | data formatting | bytes 23068672 | tf_op jit(solution)/shard_map/reshape | solution.py:16
  122.6 17.7 %all-gather.6.cloned.1.call-done = bf16[512,2048]{1,0:T(8,128)(2,1)} async-done(((bf16[256,2048]{1,0:T(8,128)(2,1)}), bf16[512,2048]{1,0:T(8,128)(2,1)}) %all-gather.6.cloned.1.call-update) | async-done | bytes 2097168 | tf_op jit(solution)/shard_map/all_gather | solution.py:96
  140.3 96.3 %all-gather.8.cloned.1.call-done = bf16[2048,2816]{1,0:T(8,128)(2,1)} async-done(((bf16[128,2816]{1,0:T(8,128)(2,1)}), bf16[2048,2816]{1,0:T(8,128)(2,1)}) %all-gather.8.cloned.1.call-update) | async-done | bytes 11534352 | tf_op jit(solution)/shard_map/all_gather | solution.py:98
  236.6 12.5 %fusion.26 = f32[512,2816]{1,0:T(8,128)} fusion(bf16[512,2048]{1,0:T(8,128)(2,1)} %all-gather.6.cloned.1.call-done, bf16[2048,2816]{1,0:T(8,128)(2,1)} %all-gather.8.cloned.1.call-done), kind=kOutput, calls=%fused_computation.44 | convolution fusion | flops 5905580032 | bytes 19398656 | tf_op jit(solution)/shard_map/dot_general | solution.py:101
  249.1 81.9 %all-gather.10.cloned.1.call-done = bf16[2048,2816]{1,0:T(8,128)(2,1)} async-done(((bf16[128,2816]{1,0:T(8,128)(2,1)}), bf16[2048,2816]{1,0:T(8,128)(2,1)}) %all-gather.10.cloned.1.call-update) | async-done | bytes 11534352 | tf_op jit(solution)/shard_map/all_gather | solution.py:99
  331.0 27.2 %convolution_convert_fusion = bf16[512,2048]{1,0:T(8,128)(2,1)} fusion(bf16[2816,2048]{0,1:T(8,128)(2,1)} %bitcast.50, f32[512,2816]{1,0:T(8,128)} %fusion.26, bf16[512,2048]{1,0:T(8,128)(2,1)} %all-gather.6.cloned.1.call-done, bf16[2048,2816]{1,0:T(8,128)(2,1)} %all-gather.10.cloned.1.call-done), kind=kOutput, calls=%fused_computation.8 | convolution fusion | flops 11820859392 | bytes 33030144 | tf_op jit(solution)/shard_map/dot_general | solution.py:104
  358.2 0.0 reduce-scatter.2.cloned.1.call-update
  358.3 30.2 %reduce-scatter.2.cloned.1.call-done = bf16[256,2048]{1,0:T(8,128)(2,1)} async-done(((bf16[512,2048]{1,0:T(8,128)(2,1)}), bf16[256,2048]{1,0:T(8,128)(2,1)}) %reduce-scatter.2.cloned.1.call-update) | async-done | bytes 1048592 | tf_op jit(solution)/shard_map/reduce_scatter | solution.py:106
  388.5 1.9 fusion.6
  390.4 0.0 copy-start.6
  390.5 0.0 copy-done
  390.5 0.8 multiply_reduce_fusion
  391.3 0.0 copy-done.6
  391.3 2.3 multiply_convert_fusion.1
  (14 shorter events, 0.1 us)
Async XLA Ops:
  6.5 19.6 %copy-start.5 = (s32[512]{0:T(512)S(1)}, s32[512]{0:T(512)}, u32[]{:S(2)}) copy-start(s32[512]{0:T(512)} %param.15) | copy-start | bytes 6148
  6.5 22.7 %copy-start.2 = (bf16[512,256]{1,0:T(8,128)(2,1)S(1)}, bf16[512,256]{1,0:T(8,128)(2,1)}, u32[]{:S(2)}) copy-start(bf16[512,256]{1,0:T(8,128)(2,1)} %param.14) | copy-start | bytes 786436
  6.5 18.1 %copy-start.3 = (bf16[512,512]{1,0:T(8,128)(2,1)S(1)}, bf16[512,512]{1,0:T(8,128)(2,1)}, u32[]{:S(2)}) copy-start(bf16[512,512]{1,0:T(8,128)(2,1)} %param.12) | copy-start | bytes 1572868
  6.5 18.2 %copy-start.7 = (f32[4]{0:T(128)S(1)}, f32[4]{0:T(128)}, u32[]{:S(2)}) copy-start(f32[4]{0:T(128)} %param.16) | copy-start | bytes 52
  6.5 100.9 %all-gather.12.cloned.1.call-start = ((), (), s32[]{:S(2)}) async-start(), calls=%async_computation.6 | async-start | bytes 12255232 | tf_op jit(solution)/shard_map/all_gather | solution.py:15
  7.3 133.0 %all-gather.6.cloned.1.call-start = ((), (), s32[]{:S(2)}) async-start(), calls=%async_computation.2 | async-start | bytes 3145728 | tf_op jit(solution)/shard_map/all_gather | solution.py:96
  8.1 16.8 %collective-permute-start.2 = (s32[128]{0:T(128)S(1)}, s32[128]{0:T(128)S(1)}, u32[]{:S(2)}, u32[]{:S(2)}) collective-permute-start(s32[128]{0:T(128)S(1)} %get-tuple-element.25), channel_id=1, source_target_pairs={{0,2},{2,4},{4,6},{6,8},{8,10},{10,12},{12,14},{14,16},{16,18},{18... | collective-permute-start | bytes 1544 | tf_op jit(solution)/shard_map/ppermute | solution.py:23
  10.5 15.7 %collective-permute-start.3 = (s32[128]{0:T(128)S(1)}, s32[128]{0:T(128)S(1)}, u32[]{:S(2)}, u32[]{:S(2)}) collective-permute-start(s32[128]{0:T(128)S(1)} %get-tuple-element.26), channel_id=1, source_target_pairs={{2,0},{4,2},{6,4},{8,6},{10,8},{12,10},{14,12},{16,14},{18,16},{20... | collective-permute-start | bytes 1544 | tf_op jit(solution)/shard_map/ppermute | solution.py:23
  12.9 16.5 %collective-permute-start.4 = (bf16[128,256]{0,1:T(8,128)(2,1)S(1)}, bf16[128,256]{0,1:T(8,128)(2,1)S(1)}, u32[]{:S(2)}, u32[]{:S(2)}) collective-permute-start(bf16[128,256]{0,1:T(8,128)(2,1)S(1)} %get-tuple-element.21), channel_id=1, source_target_pairs={{0,2},{2,4},{4,6},{6,8},{8,10},{10,12},{12,14},{14,16},{16,18},{18... | collective-permute-start | bytes 196616 | tf_op jit(solution)/shard_map/ppermute | solution.py:23
  18.1 11.4 %collective-permute-start.5 = (bf16[128,256]{0,1:T(8,128)(2,1)S(1)}, bf16[128,256]{0,1:T(8,128)(2,1)S(1)}, u32[]{:S(2)}, u32[]{:S(2)}) collective-permute-start(bf16[128,256]{0,1:T(8,128)(2,1)S(1)} %get-tuple-element.22), channel_id=1, source_target_pairs={{2,0},{4,2},{6,4},{8,6},{10,8},{12,10},{14,12},{16,14},{18,16},{20... | collective-permute-start | bytes 196616 | tf_op jit(solution)/shard_map/ppermute | solution.py:23
  20.3 6.8 %collective-permute-start = (bf16[128,256]{1,0:T(8,128)(2,1)S(1)}, bf16[128,256]{1,0:T(8,128)(2,1)S(1)}, u32[]{:S(2)}, u32[]{:S(2)}) collective-permute-start(bf16[128,256]{1,0:T(8,128)(2,1)S(1)} %get-tuple-element.23), channel_id=1, source_target_pairs={{0,2},{2,4},{4,6},{6,8},{8,10},{10,12},{12,14},{14,16},{16,18},{18... | collective-permute-start | bytes 196616 | tf_op jit(solution)/shard_map/ppermute | solution.py:23
  24.8 4.4 %collective-permute-start.1 = (bf16[128,256]{1,0:T(8,128)(2,1)S(1)}, bf16[128,256]{1,0:T(8,128)(2,1)S(1)}, u32[]{:S(2)}, u32[]{:S(2)}) collective-permute-start(bf16[128,256]{1,0:T(8,128)(2,1)S(1)} %get-tuple-element.24), channel_id=1, source_target_pairs={{2,0},{4,2},{6,4},{8,6},{10,8},{12,10},{14,12},{16,14},{18,16},{20... | collective-permute-start | bytes 196616 | tf_op jit(solution)/shard_map/ppermute | solution.py:23
  34.5 10.0 %copy-start.1 = (bf16[256,2048]{1,0:T(8,128)(2,1)S(1)}, bf16[256,2048]{1,0:T(8,128)(2,1)}, u32[]{:S(2)}) copy-start(bf16[256,2048]{1,0:T(8,128)(2,1)} %param.17) | copy-start | bytes 3145732
  48.1 0.7 copy-start.4
  50.1 186.5 %all-gather.8.cloned.1.call-start = ((), (), s32[]{:S(2)}) async-start(), calls=%async_computation.3 | async-start | bytes 12255232 | tf_op jit(solution)/shard_map/all_gather | solution.py:98
  50.9 280.2 %all-gather.10.cloned.1.call-start = ((), (), s32[]{:S(2)}) async-start(), calls=%async_computation.4 | async-start | bytes 12255232 | tf_op jit(solution)/shard_map/all_gather | solution.py:99
  51.4 337.1 %reduce-scatter.2.cloned.1.call-start = ((), (), s32[]{:S(2)}) async-start(), calls=%async_computation.5 | async-start | bytes 3145728 | tf_op jit(solution)/shard_map/reduce_scatter | solution.py:106
  388.5 2.0 copy-start
  390.4 0.8 copy-start.6
Sparse Core Ops, SparseCore 0:
  9.6 97.7 all-gather.11
  109.0 31.3 all-gather.5
  142.6 93.9 all-gather.7
  238.8 92.2 all-gather.9
  358.4 30.0 reduce-scatter.1
